TPU v7x, 32 devices: a whole 2x2x4 slice. The times are simulated.
32 devices in a mesh: ep: 8 (over z, x), tp: 4 (over y, core).
Axes of the slice: x: 2, y: 2, z: 4, core: 2. Of those that a mesh axis runs over, the one named last changes fastest.
Arguments:
- conv_value: bfloat16 [1024, 4096], P('tp', 'ep'), may hold values from -6 to 6
- conv_gate: bfloat16 [1024, 4096], P('tp', 'ep'), may hold values from -8 to 8
- conv_kernel: bfloat16 [31, 1024], P(None, 'tp'), may hold values from -1 to 1
- norm_gain: float32 [1024], replicated, may hold values from 0.1 to 1.9
- norm_shift: float32 [1024], replicated, may hold values from -3 to 3
- out_weight: bfloat16 [1024, 4096], P(None, 'tp'), may hold values from -0.1875 to 0.1875
- expert_input: bfloat16 [1024, 4096], P('ep'), may hold values from -6 to 6
- expert_ids: int32 [1024, 2], P('ep'), may hold values from 0 to 7, as said below
- pair_logits: float32 [1024, 2], P('ep'), may hold values from -6 to 6
- group_prob: float32 [1024], P('ep'), may hold values from 0.3 to 1
- expert_gate: bfloat16 [8, 4096, 2048], P('ep', None, 'tp'), may hold values from -0.09375 to 0.09375
- expert_up: bfloat16 [8, 4096, 2048], P('ep', None, 'tp'), may hold values from -0.09375 to 0.09375
- expert_down: bfloat16 [8, 2048, 4096], P('ep', None, 'tp'), may hold values from -0.125 to 0.125
Outputs:
- mixer_out: bfloat16 [4096, 4096], P('ep', 'tp')
- expert_out: bfloat16 [1024, 4096], P('ep', 'tp')
Inputs may be any that keep to these rules, and one draw needn't show every extreme that they name: `expert_ids`: the two experts of a token differ and lie in one group, ids g * 2 to (g + 1) * 2 - 1 for some g. The 128 tokens of one index of ep name every expert exactly 32 times.
All inputs are finite; a program needn't handle non-finite values.
Results may differ from a plain program's by a relative error of at most 0.0064.
Values may be sent and summed in bfloat16 or wider, within the bound.
A program may use at most 64 MiB of HBM per device.

v0:
```python
import functools

import jax
import jax.numpy as jnp
from jax import lax
from jax.experimental import pallas as pl
from jax.experimental.pallas import tpu as pltpu
from jax.sharding import PartitionSpec as P

MESH = pl.DeviceIdType.MESH
CORES = 2
F32, BF16 = jnp.float32, jnp.bfloat16


def tiles(size, most):
    tile = min(size, most)
    return tile, size // tile


def kernel(
    experts,
    parts,
    value_hbm,
    gate_hbm,
    input_hbm,
    wgate_hbm,
    wup_hbm,
    wdown_hbm,
    wout_hbm,
    taps_ref,
    gain_ref,
    shift_ref,
    ids_ref,
    logits_ref,
    prob_ref,
    mixer_hbm,
    expert_hbm,
    value,
    gate,
    tokens,
    wgate,
    wup,
    wdown,
    wout,
    send_rows,
    arrived,
    gate_sum,
    up_sum,
    hidden,
    down_sum,
    result,
    returned,
    padded,
    edges,
    halo,
    conv,
    swished,
    mixer,
    combined,
    load_sem,
    out_sem,
    self_sem,
    disp_send,
    disp_recv,
    fwd_send,
    fwd_recv,
    hal_send,
    hal_recv,
    conv_send,
    conv_recv,
    hid_send,
    hid_recv,
    ret_send,
    ret_recv,
):
    me = lax.axis_index("ep")
    tp = lax.axis_index("tp")
    chips = parts // CORES
    chip, core = lax.div(tp, CORES), lax.rem(tp, CORES)
    other = 1 - core
    sibling = chip * CORES + other
    slots = send_rows.shape[1]
    half = send_rows.shape[2]
    rows = experts * slots
    length, channels = conv.shape[1], conv.shape[2]
    edge = halo.shape[1]
    reach = (taps_ref.shape[0] - 1) // 2

    def remote(src, dst, ssem, rsem, ep=None, part=None):
        target = (me if ep is None else ep, tp if part is None else part)
        return pltpu.make_async_remote_copy(
            src_ref=src, dst_ref=dst, send_sem=ssem, recv_sem=rsem, device_id=target, device_id_type=MESH
        )

    def ahead(k):
        return lax.rem(me + k, experts)

    def behind(k):
        return lax.rem(me + experts - k, experts)

    def chip_ahead(k):
        return lax.rem(chip + k, chips) * CORES + core

    def chip_behind(k):
        return lax.rem(chip + chips - k, chips) * CORES + core

    barrier = pltpu.get_barrier_semaphore()

    @pl.loop(1, experts)
    def _(k):
        pl.semaphore_signal(barrier, inc=1, device_id=(ahead(k), tp), device_id_type=MESH)

    @pl.loop(1, chips)
    def _(k):
        pl.semaphore_signal(barrier, inc=1, device_id=(me, chip_ahead(k)), device_id_type=MESH)

    pl.semaphore_signal(barrier, inc=1, device_id=(me, sibling), device_id_type=MESH)

    columns = pl.ds(pl.multiple_of(core * half, half), half)
    loads = [
        pltpu.make_async_copy(src, dst, load_sem.at[i])
        for i, (src, dst) in enumerate(
            [
                (input_hbm.at[:, columns], tokens),
                (value_hbm, value),
                (gate_hbm, gate),
                (wgate_hbm.at[0], wgate),
                (wup_hbm.at[0], wup),
                (wout_hbm, wout),
                (wdown_hbm.at[0], wdown),
            ]
        )
    ]
    for load in loads:
        load.start()

    count = ids_ref.shape[1]
    first, second = ids_ref[0:1, :], ids_ref[1:2, :]
    expert_of = lax.broadcasted_iota(jnp.int32, (experts, count), 0)
    is_first, is_second = expert_of == first, expert_of == second
    chosen = jnp.where(is_first | is_second, 1.0, 0.0).astype(F32)
    earlier = lax.broadcasted_iota(jnp.int32, (count, count), 0) < lax.broadcasted_iota(
        jnp.int32, (count, count), 1
    )
    rank = jnp.dot(
        chosen.astype(BF16), jnp.where(earlier, 1.0, 0.0).astype(BF16), preferred_element_type=F32
    )
    rank = jnp.where(chosen > 0, rank, -1.0)
    ordinal = lax.broadcasted_iota(jnp.int32, (experts, slots, count), 1).astype(F32)
    place3 = jnp.broadcast_to(rank[:, None, :], (experts, slots, count)) == ordinal
    place = jnp.where(place3, 1.0, 0.0).astype(F32).reshape(rows, count)

    loads[0].wait()
    tile, steps = tiles(half, 512)
    for i in range(steps):
        span = slice(i * tile, (i + 1) * tile)
        picked = jnp.dot(place.astype(BF16), tokens[:, span], preferred_element_type=F32)
        send_rows[:, :, span] = picked.reshape(experts, slots, tile).astype(BF16)

    pl.semaphore_wait(barrier, experts - 1 + chips)

    def dispatch(k):
        return remote(
            send_rows.at[ahead(k)], arrived.at[core, me], disp_send.at[k], disp_recv.at[k], ep=ahead(k)
        )

    def forward(k, src):
        return remote(
            src, arrived.at[core, behind(k)], fwd_send.at[k], fwd_recv.at[k], part=sibling
        )

    @pl.loop(1, experts)
    def _(k):
        dispatch(k).start()

    keep = pltpu.make_async_copy(send_rows.at[me], arrived.at[core, me], self_sem.at[0])
    keep.start()
    forward(0, send_rows.at[me]).start()

    loads[1].wait()
    loads[2].wait()
    gated = (value[...].astype(F32) * jax.nn.sigmoid(gate[...].astype(F32))).astype(BF16)
    padded[edge : edge + length, :] = jnp.transpose(gated.astype(F32), (1, 0))
    edges[0] = padded[edge : 2 * edge, :].astype(BF16)
    edges[1] = padded[length : length + edge, :].astype(BF16)
    to_left = remote(edges.at[0], halo.at[1], hal_send.at[0], hal_recv.at[0], ep=behind(1))
    to_right = remote(edges.at[1], halo.at[0], hal_send.at[1], hal_recv.at[1], ep=ahead(1))
    to_left.start()
    to_right.start()
    taps = taps_ref[...].astype(F32)
    chunk, chunks = tiles(length, 64)

    def convolve(i):
        total = jnp.zeros((chunk, channels), F32)
        for j in range(taps.shape[0]):
            start = i * chunk + j + edge - reach
            total = total + taps[j : j + 1, :] * padded[start : start + chunk, :]
        conv[tp, i * chunk : (i + 1) * chunk, :] = total.astype(BF16)

    for i in range(1, chunks - 1):
        convolve(i)
    to_left.wait()
    to_right.wait()
    padded[0:edge, :] = jnp.where(me == 0, 0.0, halo[0].astype(F32))
    padded[edge + length : 2 * edge + length, :] = jnp.where(
        me == experts - 1, 0.0, halo[1].astype(F32)
    )
    convolve(0)
    convolve(chunks - 1)

    def gather(buffer, ssem, rsem):
        def across(k):
            return remote(buffer.at[tp], buffer.at[tp], ssem.at[k], rsem.at[k], part=chip_ahead(k))

        def beside(k):
            block = chip_behind(k)
            return remote(
                buffer.at[block], buffer.at[block], ssem.at[chips + k], rsem.at[chips + k], part=sibling
            )

        return across, beside

    conv_across, conv_beside = gather(conv, conv_send, conv_recv)

    @pl.loop(1, chips)
    def _(k):
        conv_across(k).start()

    conv_beside(0).start()

    @pl.loop(1, experts)
    def _(k):
        dispatch(k).wait_recv()
        forward(k, arrived.at[core, behind(k)]).start()

    keep.wait()
    loads[3].wait()
    loads[4].wait()
    units = gate_sum.shape[1]
    tile, steps = tiles(units, 256)

    def side(which):
        block = arrived[which]
        if slots % 16:
            return block.astype(F32).reshape(rows, half).astype(BF16)
        return block.reshape(rows, half)

    def depth(which):
        return pl.ds(pl.multiple_of(which * half, half), half)

    for i in range(steps):
        span = slice(i * tile, (i + 1) * tile)
        gate_sum[:, span] = jnp.dot(side(core), wgate[depth(core), span], preferred_element_type=F32)
        up_sum[:, span] = jnp.dot(side(core), wup[depth(core), span], preferred_element_type=F32)

    @pl.loop(0, experts)
    def _(k):
        forward(k, send_rows.at[me]).wait_recv()

    for i in range(steps):
        span = slice(i * tile, (i + 1) * tile)
        gate_val = gate_sum[:, span] + jnp.dot(
            side(other), wgate[depth(other), span], preferred_element_type=F32
        )
        up_val = up_sum[:, span] + jnp.dot(
            side(other), wup[depth(other), span], preferred_element_type=F32
        )
        hidden[tp, :, span] = (jax.nn.silu(gate_val) * up_val).astype(BF16)

    hid_across, hid_beside = gather(hidden, hid_send, hid_recv)

    @pl.loop(1, chips)
    def _(k):
        hid_across(k).start()

    hid_beside(0).start()

    @pl.loop(1, chips)
    def _(k):
        conv_across(k).wait_recv()
        conv_beside(k).start()

    @pl.loop(0, chips)
    def _(k):
        conv_beside(k).wait_recv()

    width = parts * channels
    chunk, chunks = tiles(length, 64)

    @pl.loop(0, chunks)
    def _(i):
        span = pl.ds(pl.multiple_of(i * chunk, chunk), chunk)
        blocks = [conv[b, span, :].astype(F32) for b in range(parts)]
        center = sum(jnp.sum(block, axis=1, keepdims=True) for block in blocks) / width
        blocks = [block - center for block in blocks]
        spread = sum(jnp.sum(block * block, axis=1, keepdims=True) for block in blocks) / width
        scale = lax.rsqrt(spread + 1e-05)
        for b in range(parts):
            lanes = slice(b * channels, (b + 1) * channels)
            normed = blocks[b] * scale * gain_ref[:, lanes] + shift_ref[:, lanes]
            swished[b, span, :] = jax.nn.silu(normed).astype(BF16)

    loads[6].wait()
    wide = down_sum.shape[1]
    tile, steps = tiles(wide, 256)

    def down(block, begin):
        deep = pl.ds(pl.multiple_of(block * units, units), units)

        @pl.loop(0, steps)
        def _(i):
            span = pl.ds(pl.multiple_of(i * tile, tile), tile)
            product = jnp.dot(hidden[block], wdown[deep, span], preferred_element_type=F32)
            down_sum[:, span] = product if begin else down_sum[:, span] + product

    down(tp, True)
    hid_beside(0).wait_recv()
    down(sibling, False)

    @pl.loop(1, chips)
    def _(k):
        hid_across(k).wait_recv()
        hid_beside(k).start()
        down(chip_behind(k), False)
        hid_beside(k).wait_recv()
        down(chip_behind(k) + other - core, False)

    result[...] = down_sum[...].reshape(experts, slots, wide).astype(BF16)

    def give_back(k):
        return remote(result.at[ahead(k)], returned.at[me], ret_send.at[k], ret_recv.at[k], ep=ahead(k))

    @pl.loop(1, experts)
    def _(k):
        give_back(k).start()

    own = pltpu.make_async_copy(result.at[me], returned.at[me], self_sem.at[1])
    own.start()

    loads[5].wait()
    tile, steps = tiles(mixer.shape[1], 256)

    @pl.loop(0, steps)
    def _(i):
        span = pl.ds(pl.multiple_of(i * tile, tile), tile)
        total = jnp.zeros((length, tile), F32)
        for b in range(parts):
            total = total + jnp.dot(
                swished[b], wout[b * channels : (b + 1) * channels, span], preferred_element_type=F32
            )
        mixer[:, span] = total.astype(BF16)

    put_mixer = pltpu.make_async_copy(mixer, mixer_hbm, out_sem.at[0])
    put_mixer.start()

    share = jax.nn.sigmoid(logits_ref[0:1, :] - logits_ref[1:2, :])
    weight = jnp.where(is_first, share * prob_ref[...], 0.0) + jnp.where(
        is_second, (1.0 - share) * prob_ref[...], 0.0
    )
    weights = jnp.where(
        place3, jnp.broadcast_to(weight[:, None, :], (experts, slots, count)), 0.0
    ).reshape(rows, count)
    weights = jnp.transpose(weights, (1, 0))
    high = weights.astype(BF16)
    rest = weights - high.astype(F32)
    middle = rest.astype(BF16)
    low = (rest - middle.astype(F32)).astype(BF16)

    own.wait()

    @pl.loop(1, experts)
    def _(k):
        give_back(k).wait_recv()

    tile, steps = tiles(wide, 512)
    for i in range(steps):
        span = slice(i * tile, (i + 1) * tile)
        block = returned[:, :, span]
        if slots % 16:
            block = block.astype(F32).reshape(rows, tile).astype(BF16)
        else:
            block = block.reshape(rows, tile)
        total = jnp.dot(low, block, preferred_element_type=F32)
        total = total + jnp.dot(middle, block, preferred_element_type=F32)
        total = total + jnp.dot(high, block, preferred_element_type=F32)
        combined[:, span] = total.astype(BF16)

    put_expert = pltpu.make_async_copy(combined, expert_hbm, out_sem.at[1])
    put_expert.start()

    @pl.loop(1, experts)
    def _(k):
        dispatch(k).wait_send()
        give_back(k).wait_send()

    @pl.loop(0, experts)
    def _(k):
        forward(k, send_rows.at[me]).wait_send()

    @pl.loop(1, chips)
    def _(k):
        conv_across(k).wait_send()
        hid_across(k).wait_send()

    @pl.loop(0, chips)
    def _(k):
        conv_beside(k).wait_send()
        hid_beside(k).wait_send()

    put_mixer.wait()
    put_expert.wait()


def local(
    experts,
    parts,
    conv_value,
    conv_gate,
    conv_kernel,
    norm_gain,
    norm_shift,
    out_weight,
    expert_input,
    expert_ids,
    pair_logits,
    group_prob,
    expert_gate,
    expert_up,
    expert_down,
):
    channels, length = conv_value.shape
    count, model = expert_input.shape
    slots = 2 * count // experts
    rows = experts * slots
    half = model // CORES
    units, wide = expert_gate.shape[2], expert_down.shape[2]
    out_width = out_weight.shape[1]
    chips = parts // CORES
    edge = -(-((conv_kernel.shape[0] - 1) // 2) // 16) * 16
    anywhere = pl.BlockSpec(memory_space=pl.ANY)
    near = pl.BlockSpec(memory_space=pltpu.VMEM)
    dma = pltpu.SemaphoreType.DMA
    return pl.pallas_call(
        functools.partial(kernel, experts, parts),
        out_shape=(
            pltpu.VMEM((length, out_width), BF16),
            pltpu.VMEM((count, wide), BF16),
        ),
        in_specs=[anywhere] * 7 + [near] * 6,
        out_specs=(anywhere, anywhere),
        scratch_shapes=[
            pltpu.VMEM((channels, length), BF16),
            pltpu.VMEM((channels, length), BF16),
            pltpu.VMEM((count, half), BF16),
            pltpu.VMEM((model, units), BF16),
            pltpu.VMEM((model, units), BF16),
            pltpu.VMEM(expert_down.shape[1:], BF16),
            pltpu.VMEM(out_weight.shape, BF16),
            pltpu.VMEM((experts, slots, half), BF16),
            pltpu.VMEM((CORES, experts, slots, half), BF16),
            pltpu.VMEM((rows, units), F32),
            pltpu.VMEM((rows, units), F32),
            pltpu.VMEM((parts, rows, units), BF16),
            pltpu.VMEM((rows, wide), F32),
            pltpu.VMEM((experts, slots, wide), BF16),
            pltpu.VMEM((experts, slots, wide), BF16),
            pltpu.VMEM((length + 2 * edge, channels), F32),
            pltpu.VMEM((2, edge, channels), BF16),
            pltpu.VMEM((2, edge, channels), BF16),
            pltpu.VMEM((parts, length, channels), BF16),
            pltpu.VMEM((parts, length, channels), BF16),
            pltpu.VMEM((length, out_width), BF16),
            pltpu.VMEM((count, wide), BF16),
            dma((7,)),
            dma((2,)),
            dma((2,)),
            dma((experts,)),
            dma((experts,)),
            dma((experts,)),
            dma((experts,)),
            dma((2,)),
            dma((2,)),
            dma((2 * chips,)),
            dma((2 * chips,)),
            dma((2 * chips,)),
            dma((2 * chips,)),
            dma((experts,)),
            dma((experts,)),
        ],
        compiler_params=pltpu.CompilerParams(
            collective_id=0, has_side_effects=True, vmem_limit_bytes=60 * 1024 * 1024
        ),
        name="block",
    )(
        conv_value,
        conv_gate,
        expert_input,
        expert_gate,
        expert_up,
        expert_down,
        out_weight,
        conv_kernel,
        norm_gain[None, :],
        norm_shift[None, :],
        expert_ids.T,
        pair_logits.T,
        group_prob[None, :],
    )


def solution(mesh):
    placed = (
        P("tp", "ep"),
        P("tp", "ep"),
        P(None, "tp"),
        P(),
        P(),
        P(None, "tp"),
        P("ep", None),
        P("ep", None),
        P("ep", None),
        P("ep"),
        P("ep", None, "tp"),
        P("ep", None, "tp"),
        P("ep", None, "tp"),
    )
    return jax.shard_map(
        functools.partial(local, mesh.shape["ep"], mesh.shape["tp"]),
        mesh=mesh,
        in_specs=placed,
        out_specs=(P("ep", "tp"), P("ep", "tp")),
        check_vma=False,
    )
```

profile of v0, /device:TPU:11, one launch (start us, length us, event | category | flops | bytes accessed | tf_op | source)
XLA Modules:
  0.0 58.2 jit_solution(6203152134228498729)
XLA Ops:
  0.6 55.9 %block.1 = (bf16[512,1024]{1,0:T(8,128)(2,1)S(1)}, bf16[128,1024]{1,0:T(8,128)(2,1)S(1)}) custom-call(bf16[256,512]{1,0:T(8,128)(2,1)} %value_hbm.1, bf16[256,512]{1,0:T(8,128)(2,1)} %gate_hbm.1, bf16[128,4096]{1,0:T(8,128)(2,1)} %input_hbm.1, bf16[1,4096,512]{2,1,0:T(8,128)(2,1)} %wgate_hbm.1, bf16[1,4096,512]{2,1,0:T(8,128)(2,1)} %wup_hbm.1, ...), custom_call_target="tpu_custom_call" | custom-call | tf_op jit(solution)/shard_map/block/pallas_call | solution.py:443
  56.5 1.0 %copy.17 = bf16[512,1024]{1,0:T(8,128)(2,1)} copy(bf16[512,1024]{1,0:T(8,128)(2,1)S(1)} %get-tuple-element.2) | data formatting | bytes 2097152
  57.5 0.7 %copy.18 = bf16[128,1024]{1,0:T(8,128)(2,1)} copy(bf16[128,1024]{1,0:T(8,128)(2,1)S(1)} %get-tuple-element.3) | data formatting | bytes 524288
where the time goes:
time: 58.4 us; the launch traced here: 58.2 us
  Pallas kernels  55.9 us (96%)
  local copies, waits for them, and re-layouts  1.67 us (3%)
  between operations  0.64 us (1%)
    pallas_call x1, Pallas kernels, local(): pl.pallas_call(functools.partial(kernel, experts, parts), out_shape=(pltp...  55.9 us
    unnamed x2, local copies, waits for them, and re-layouts  1.67 us

commit v1 on v0

--- a/solution.py
+++ b/solution.py
@@ -9,6 +9,8 @@
 
 MESH = pl.DeviceIdType.MESH
 CORES = 2
+PAIR = 2
+GROUPS = 4
 F32, BF16 = jnp.float32, jnp.bfloat16
 
 
@@ -411,6 +413,595 @@
     put_expert.wait()
 
 
+def pair_kernel(
+    groups,
+    parts,
+    value_hbm,
+    gate_hbm,
+    input_hbm,
+    wgate_hbm,
+    wup_hbm,
+    wdown_hbm,
+    wout_hbm,
+    taps_ref,
+    gain_ref,
+    shift_ref,
+    ids_ref,
+    logits_ref,
+    prob_ref,
+    mixer,
+    combined,
+    value,
+    gate,
+    mine,
+    tokens,
+    wgate,
+    wup,
+    wdown,
+    wout,
+    send_rows,
+    weights,
+    arrived_weights,
+    arrived,
+    gate_sum,
+    up_sum,
+    hidden,
+    down_sum,
+    result,
+    other_result,
+    summed,
+    returned,
+    scatter,
+    padded,
+    edges,
+    halo,
+    conv,
+    swished,
+    load_sem,
+    z_send,
+    z_recv,
+    w_send,
+    w_recv,
+    y_send,
+    y_recv,
+    x_send,
+    x_recv,
+    d_send,
+    d_recv,
+    s_send,
+    s_recv,
+    hal_send,
+    hal_recv,
+    conv_send,
+    conv_recv,
+    hid_send,
+    hid_recv,
+    res_send,
+    res_recv,
+    ret_send,
+    ret_recv,
+):
+    experts = groups * PAIR
+    me = lax.axis_index("ep")
+    tp = lax.axis_index("tp")
+    group, side = lax.div(me, PAIR), lax.rem(me, PAIR)
+    mate = group * PAIR + 1 - side
+    chip, core = lax.div(tp, CORES), lax.rem(tp, CORES)
+    sibling = chip * CORES + 1 - core
+    beside = (1 - chip) * CORES + core
+    opposite = (1 - chip) * CORES + 1 - core
+    slots, quarter = send_rows.shape[1], send_rows.shape[2]
+    order = list(range(0, groups, 2)) + list(range(1, groups, 2))
+    spans = 2
+    per = groups // spans
+    rows = per * PAIR * slots
+    length, channels = conv.shape[1], conv.shape[2]
+    edge = halo.shape[1]
+    reach = (taps_ref.shape[0] - 1) // 2
+
+    def remote(src, dst, ssem, rsem, ep=None, part=None):
+        target = (me if ep is None else ep, tp if part is None else part)
+        return pltpu.make_async_remote_copy(
+            src_ref=src, dst_ref=dst, send_sem=ssem, recv_sem=rsem, device_id=target, device_id_type=MESH
+        )
+
+    def onward(k):
+        return lax.rem(group + k, groups) * PAIR + side
+
+    def backward(k):
+        return lax.rem(group + groups - k, groups) * PAIR + side
+
+    left, right = lax.rem(me + experts - 1, experts), lax.rem(me + 1, experts)
+    barrier = pltpu.get_barrier_semaphore()
+    peers = [(onward(k), tp) for k in range(1, groups)]
+    peers += [(mate, tp), (me, beside), (me, sibling), (left, tp), (right, tp)]
+    for peer in peers:
+        pl.semaphore_signal(barrier, inc=1, device_id=peer, device_id_type=MESH)
+
+    columns = pl.ds(pl.multiple_of(tp * quarter, quarter), quarter)
+    loads = [
+        pltpu.make_async_copy(src, dst, load_sem.at[i])
+        for i, (src, dst) in enumerate(
+            [
+                (input_hbm.at[:, columns], mine),
+                (input_hbm, tokens),
+                (value_hbm, value),
+                (gate_hbm, gate),
+                (wgate_hbm.at[0], wgate),
+                (wup_hbm.at[0], wup),
+                (wdown_hbm.at[0], wdown),
+                (wout_hbm, wout),
+            ]
+        )
+    ]
+    for load in loads:
+        load.start()
+
+    count = ids_ref.shape[1]
+    first, second = ids_ref[0:1, :], ids_ref[1:2, :]
+    position = lax.broadcasted_iota(jnp.int32, (groups, count), 0) + group
+    position = jnp.where(position >= groups, position - groups, position) * PAIR
+    chosen = jnp.where((first >= position) & (first < position + PAIR), 1.0, 0.0).astype(F32)
+    earlier = lax.broadcasted_iota(jnp.int32, (count, count), 0) < lax.broadcasted_iota(
+        jnp.int32, (count, count), 1
+    )
+    rank = jnp.dot(
+        chosen.astype(BF16), jnp.where(earlier, 1.0, 0.0).astype(BF16), preferred_element_type=F32
+    )
+    rank = jnp.where(chosen > 0, rank, -1.0)
+    ordinal = lax.broadcasted_iota(jnp.int32, (groups, slots, count), 1).astype(F32)
+    place3 = jnp.broadcast_to(rank[:, None, :], (groups, slots, count)) == ordinal
+    place_f = jnp.where(place3, 1.0, 0.0).astype(F32).reshape(groups * slots, count)
+    place = place_f.astype(BF16)
+
+    def dispatch(k):
+        return remote(
+            send_rows.at[k - 1],
+            arrived.at[tp, order.index(k), 0],
+            z_send.at[k],
+            z_recv.at[k],
+            ep=onward(k),
+        )
+
+    loads[0].wait()
+    picked = jnp.dot(place[slots:], mine[...], preferred_element_type=F32)
+    send_rows[...] = picked.astype(BF16).reshape(groups - 1, slots, quarter)
+    pl.semaphore_wait(barrier, len(peers))
+    for k in order[1:]:
+        dispatch(k).start()
+
+    def to_beside(p):
+        return remote(
+            arrived.at[tp, p, 0], arrived.at[tp, p, 0], y_send.at[p], y_recv.at[p], part=beside
+        )
+
+    def to_mate(p):
+        return remote(arrived.at[tp, p, 0], arrived.at[tp, p, 1], x_send.at[p], x_recv.at[p], ep=mate)
+
+    def across(p):
+        if p == 0:
+            return remote(
+                arrived.at[beside, 0, 0], arrived.at[beside, 0, 1], d_send.at[0], d_recv.at[0], ep=mate
+            )
+        lead = core == 0
+        block = jnp.where(lead, tp, beside)
+        return remote(
+            arrived.at[block, p, 1 - core],
+            arrived.at[block, p, 1],
+            d_send.at[p],
+            d_recv.at[p],
+            ep=jnp.where(lead, me, mate),
+            part=jnp.where(lead, beside, tp),
+        )
+
+    def to_sibling(p, far, which):
+        block = beside if far else tp
+        i = 4 * p + 2 * which + far
+        return remote(
+            arrived.at[block, p, which], arrived.at[block, p, which], s_send.at[i], s_recv.at[i], part=sibling
+        )
+
+    loads[1].wait()
+    for q in range(parts):
+        picked = jnp.dot(
+            place[:slots], tokens[:, q * quarter : (q + 1) * quarter], preferred_element_type=F32
+        )
+        arrived[q, 0, 0] = picked.astype(BF16)
+    to_mate(0).start()
+    across(0).start()
+
+    share = jax.nn.sigmoid(logits_ref[0:1, :] - logits_ref[1:2, :])
+    of_first = share * prob_ref[...]
+    of_second = (1.0 - share) * prob_ref[...]
+    first_mine = (first < second) == (side == 0)
+    own_weight = jnp.sum(place_f * jnp.where(first_mine, of_first, of_second), axis=1, keepdims=True)
+    mate_weight = jnp.sum(place_f * jnp.where(first_mine, of_second, of_first), axis=1, keepdims=True)
+    lane = lax.broadcasted_iota(jnp.int32, (groups * slots, weights.shape[2]), 1)
+    both = jnp.where(lane < weights.shape[2] // 2, own_weight, mate_weight)
+    weights[...] = both.reshape(weights.shape)
+
+    def give_weights(k):
+        return remote(weights.at[k], arrived_weights.at[k], w_send.at[k], w_recv.at[k], ep=onward(k))
+
+    for k in order[1:]:
+        give_weights(k).start()
+    arrived_weights[0] = weights[0]
+    scatter[...] = jnp.transpose(place_f, (1, 0)).astype(BF16)
+
+    loads[2].wait()
+    loads[3].wait()
+    gated = (value[...].astype(F32) * jax.nn.sigmoid(gate[...].astype(F32))).astype(BF16)
+    padded[edge : edge + length, :] = jnp.transpose(gated.astype(F32), (1, 0))
+    edges[0] = padded[edge : 2 * edge, :].astype(BF16)
+    edges[1] = padded[length : length + edge, :].astype(BF16)
+    to_left = remote(edges.at[0], halo.at[1], hal_send.at[0], hal_recv.at[0], ep=left)
+    to_right = remote(edges.at[1], halo.at[0], hal_send.at[1], hal_recv.at[1], ep=right)
+    to_left.start()
+    to_right.start()
+    taps = taps_ref[...].astype(F32)
+    chunk, chunks = tiles(length, 64)
+
+    def convolve(i):
+        total = jnp.zeros((chunk, channels), F32)
+        for j in range(taps.shape[0]):
+            start = i * chunk + j + edge - reach
+            total = total + taps[j : j + 1, :] * padded[start : start + chunk, :]
+        conv[tp, i * chunk : (i + 1) * chunk, :] = total.astype(BF16)
+
+    def landed(p):
+        dispatch(order[p]).wait_recv()
+        to_beside(p).start()
+        to_mate(p).start()
+        to_sibling(p, 0, 0).start()
+
+    def turned(p):
+        if p:
+            to_beside(p).wait_recv()
+        to_mate(p).wait_recv()
+        if p:
+            across(p).start()
+            to_sibling(p, 1, 0).start()
+        to_sibling(p, 0, 1).start()
+
+    def closed(p):
+        across(p).wait_recv()
+        to_sibling(p, 1, 1).start()
+
+    inner = list(range(1, chunks - 1))
+    early = inner[: len(inner) // 3]
+    middle = inner[len(inner) // 3 : 2 * len(inner) // 3]
+    late = inner[2 * len(inner) // 3 :]
+    for i in early:
+        convolve(i)
+    landed(1)
+    turned(0)
+    for i in middle:
+        convolve(i)
+    closed(0)
+    for p in range(2, groups):
+        landed(p)
+    for i in late:
+        convolve(i)
+    turned(1)
+    to_left.wait()
+    to_right.wait()
+    padded[0:edge, :] = jnp.where(me == 0, 0.0, halo[0].astype(F32))
+    padded[edge + length : 2 * edge + length, :] = jnp.where(
+        me == experts - 1, 0.0, halo[1].astype(F32)
+    )
+    convolve(0)
+    turned(2)
+    convolve(chunks - 1)
+    for p in range(3, groups):
+        turned(p)
+
+    cuts = 2
+    share_rows = length // cuts
+
+    def conv_copy(i, kind):
+        cut = pl.ds(i * share_rows, share_rows)
+        block = beside if kind == 2 else tp
+        j = 3 * i + kind
+        return remote(
+            conv.at[block, cut],
+            conv.at[block, cut],
+            conv_send.at[j],
+            conv_recv.at[j],
+            part=beside if kind == 0 else sibling,
+        )
+
+    for i in range(cuts):
+        conv_copy(i, 1).start()
+    for p in range(1, per):
+        closed(p)
+
+    units = hidden.shape[3]
+    tile, steps = tiles(units, 256)
+
+    def gather_rows(q, h):
+        return arrived[q, h * per : (h + 1) * per].reshape(rows, quarter)
+
+    def deep(q):
+        return pl.ds(pl.multiple_of(q * quarter, quarter), quarter)
+
+    def project(h, blocks, begin):
+        for i in range(steps):
+            span = slice(i * tile, (i + 1) * tile)
+            for weight, total in ((wgate, gate_sum), (wup, up_sum)):
+                value = sum(
+                    jnp.dot(gather_rows(q, h), weight[deep(q), span], preferred_element_type=F32)
+                    for q in blocks
+                )
+                total[:, span] = value if begin else total[:, span] + value
+
+    def hid_copy(h, kind):
+        block = beside if kind == 2 else tp
+        j = 3 * h + kind
+        return remote(
+            hidden.at[h, block],
+            hidden.at[h, block],
+            hid_send.at[j],
+            hid_recv.at[j],
+            part=beside if kind == 0 else sibling,
+        )
+
+    def activate(h):
+        hidden[h, tp] = (jax.nn.silu(gate_sum[...]) * up_sum[...]).astype(BF16)
+        hid_copy(h, 0).start()
+        hid_copy(h, 1).start()
+
+    def from_sibling(h):
+        for p in range(h * per, (h + 1) * per):
+            for which in range(2):
+                for far in range(2):
+                    if p or which:
+                        to_sibling(p, far, which).wait_recv()
+
+    loads[4].wait()
+    loads[5].wait()
+    project(0, (tp, beside), True)
+    for p in range(per, groups - 1):
+        closed(p)
+    from_sibling(0)
+    project(0, (sibling, opposite), False)
+    activate(0)
+    closed(groups - 1)
+    project(1, (tp, beside), True)
+    from_sibling(1)
+    project(1, (sibling, opposite), False)
+    activate(1)
+    for i in range(cuts):
+        conv_copy(i, 0).start()
+
+    loads[6].wait()
+    wide = down_sum.shape[2]
+    pieces = result.shape[1]
+    span_wide = wide // pieces
+
+    def down(h, block, span):
+        depth = pl.ds(pl.multiple_of(block * units, units), units)
+        return jnp.dot(hidden[h, block], wdown[depth, span], preferred_element_type=F32)
+
+    def down_near(h):
+        hid_copy(h, 1).wait_recv()
+        for c in range(pieces):
+            span = slice(c * span_wide, (c + 1) * span_wide)
+            down_sum[h, :, span] = down(h, tp, span) + down(h, sibling, span)
+
+    def exchange(h, c):
+        return remote(
+            result.at[h, c, 1], other_result.at[h, c], res_send.at[2 * h + c], res_recv.at[2 * h + c], ep=mate
+        )
+
+    def down_far(h):
+        hid_copy(h, 0).wait_recv()
+        hid_copy(h, 2).start()
+        for c in range(pieces):
+            span = slice(c * span_wide, (c + 1) * span_wide)
+            total = down_sum[h, :, span] + down(h, beside, span)
+            if c == 0:
+                hid_copy(h, 2).wait_recv()
+            total = (total + down(h, opposite, span)).astype(BF16).reshape(per, PAIR, slots, span_wide)
+            for which in range(PAIR):
+                result[h, c, which] = total[:, which]
+            exchange(h, c).start()
+
+    def give_back(k, c):
+        p = order.index(k)
+        return remote(
+            summed.at[p // per, c, p % per],
+            returned.at[c, k],
+            ret_send.at[c * groups + k],
+            ret_recv.at[c * groups + k],
+            ep=backward(k),
+        )
+
+    def combine(h, c):
+        exchange(h, c).wait_recv()
+        for i in range(per):
+            k = order[h * per + i]
+            if k and c == 0:
+                give_weights(k).wait_recv()
+            half = weights.shape[2] // 2
+            ours = arrived_weights[k, :, 0:1]
+            theirs = arrived_weights[k, :, half : half + 1]
+            total = ours * result[h, c, 0, i].astype(F32) + theirs * other_result[h, c, i].astype(F32)
+            if k:
+                summed[h, c, i] = total.astype(BF16)
+                give_back(k, c).start()
+            else:
+                returned[c, 0] = total.astype(BF16)
+
+    width = parts * channels
+    norm_chunk, norm_chunks = tiles(share_rows, 64)
+
+    def normalize(cut):
+        @pl.loop(0, norm_chunks)
+        def _(i):
+            span = pl.ds(pl.multiple_of(cut * share_rows + i * norm_chunk, norm_chunk), norm_chunk)
+            blocks = [conv[b, span, :].astype(F32) for b in range(parts)]
+            center = sum(jnp.sum(block, axis=1, keepdims=True) for block in blocks) / width
+            blocks = [block - center for block in blocks]
+            spread = sum(jnp.sum(block * block, axis=1, keepdims=True) for block in blocks) / width
+            scale = lax.rsqrt(spread + 1e-05)
+            for b in range(parts):
+                lanes = slice(b * channels, (b + 1) * channels)
+                normed = blocks[b] * scale * gain_ref[:, lanes] + shift_ref[:, lanes]
+                swished[b, span, :] = jax.nn.silu(normed).astype(BF16)
+
+    out_tile, out_steps = tiles(mixer.shape[1], 256)
+
+    def mix(cut):
+        cut_rows = pl.ds(cut * share_rows, share_rows)
+
+        @pl.loop(0, out_steps)
+        def _(i):
+            span = pl.ds(pl.multiple_of(i * out_tile, out_tile), out_tile)
+            total = jnp.zeros((share_rows, out_tile), F32)
+            for b in range(parts):
+                total = total + jnp.dot(
+                    swished[b, cut_rows], wout[b * channels : (b + 1) * channels, span], preferred_element_type=F32
+                )
+            mixer[cut_rows, span] = total.astype(BF16)
+
+    down_near(0)
+    down_far(0)
+    down_near(1)
+    down_far(1)
+    for c in range(pieces):
+        combine(0, c)
+    for i in range(cuts):
+        conv_copy(i, 1).wait_recv()
+    conv_copy(0, 0).wait_recv()
+    conv_copy(0, 2).start()
+    for c in range(pieces):
+        combine(1, c)
+    loads[7].wait()
+    conv_copy(0, 2).wait_recv()
+    normalize(0)
+    mix(0)
+    for i in range(1, cuts):
+        conv_copy(i, 0).wait_recv()
+        conv_copy(i, 2).start()
+    for i in range(1, cuts):
+        conv_copy(i, 2).wait_recv()
+        normalize(i)
+        mix(i)
+    for c in range(pieces):
+        for k in range(1, groups):
+            give_back(k, c).wait_recv()
+        block = returned[c].reshape(groups * slots, span_wide)
+        combined[:, c * span_wide : (c + 1) * span_wide] = jnp.dot(
+            scatter[...], block, preferred_element_type=F32
+        ).astype(BF16)
+
+    for k in range(1, groups):
+        dispatch(k).wait_send()
+        give_weights(k).wait_send()
+        for c in range(pieces):
+            give_back(k, c).wait_send()
+    for p in range(groups):
+        if p:
+            to_beside(p).wait_send()
+        to_mate(p).wait_send()
+        across(p).wait_send()
+        for which in range(2):
+            for far in range(2):
+                if p or which:
+                    to_sibling(p, far, which).wait_send()
+    for kind in range(3):
+        for i in range(cuts):
+            conv_copy(i, kind).wait_send()
+        for h in range(spans):
+            hid_copy(h, kind).wait_send()
+    for h in range(spans):
+        for c in range(pieces):
+            exchange(h, c).wait_send()
+
+
+def pair_call(groups, parts, args):
+    conv_value, expert_input, expert_gate, expert_down = args[0], args[2], args[3], args[5]
+    out_weight, conv_kernel = args[6], args[7]
+    channels, length = conv_value.shape
+    count, model = expert_input.shape
+    slots = count // groups
+    quarter = model // parts
+    units, wide = expert_gate.shape[2], expert_down.shape[2]
+    out_width = out_weight.shape[1]
+    edge = -(-((conv_kernel.shape[0] - 1) // 2) // 16) * 16
+    spans, cuts, pieces = 2, 2, 2
+    per = groups // spans
+    rows = per * PAIR * slots
+    piece = wide // pieces
+    anywhere = pl.BlockSpec(memory_space=pl.ANY)
+    near = pl.BlockSpec(memory_space=pltpu.VMEM)
+    dma = pltpu.SemaphoreType.DMA
+    return pl.pallas_call(
+        functools.partial(pair_kernel, groups, parts),
+        out_shape=(
+            pltpu.VMEM((length, out_width), BF16),
+            pltpu.VMEM((count, wide), BF16),
+        ),
+        in_specs=[anywhere] * 7 + [near] * 6,
+        out_specs=(near, near),
+        scratch_shapes=[
+            pltpu.VMEM((channels, length), BF16),
+            pltpu.VMEM((channels, length), BF16),
+            pltpu.VMEM((count, quarter), BF16),
+            pltpu.VMEM((count, model), BF16),
+            pltpu.VMEM((model, units), BF16),
+            pltpu.VMEM((model, units), BF16),
+            pltpu.VMEM(expert_down.shape[1:], BF16),
+            pltpu.VMEM(out_weight.shape, BF16),
+            pltpu.VMEM((groups - 1, slots, quarter), BF16),
+            pltpu.VMEM((groups, slots, 128), F32),
+            pltpu.VMEM((groups, slots, 128), F32),
+            pltpu.VMEM((parts, groups, PAIR, slots, quarter), BF16),
+            pltpu.VMEM((rows, units), F32),
+            pltpu.VMEM((rows, units), F32),
+            pltpu.VMEM((spans, parts, rows, units), BF16),
+            pltpu.VMEM((spans, rows, wide), F32),
+            pltpu.VMEM((spans, pieces, PAIR, per, slots, piece), BF16),
+            pltpu.VMEM((spans, pieces, per, slots, piece), BF16),
+            pltpu.VMEM((spans, pieces, per, slots, piece), BF16),
+            pltpu.VMEM((pieces, groups, slots, piece), BF16),
+            pltpu.VMEM((count, groups * slots), BF16),
+            pltpu.VMEM((length + 2 * edge, channels), F32),
+            pltpu.VMEM((2, edge, channels), BF16),
+            pltpu.VMEM((2, edge, channels), BF16),
+            pltpu.VMEM((parts, length, channels), BF16),
+            pltpu.VMEM((parts, length, channels), BF16),
+            dma((8,)),
+            dma((groups,)),
+            dma((groups,)),
+            dma((groups,)),
+            dma((groups,)),
+            dma((groups,)),
+            dma((groups,)),
+            dma((groups,)),
+            dma((groups,)),
+            dma((groups,)),
+            dma((groups,)),
+            dma((4 * groups,)),
+            dma((4 * groups,)),
+            dma((2,)),
+            dma((2,)),
+            dma((3 * cuts,)),
+            dma((3 * cuts,)),
+            dma((3 * spans,)),
+            dma((3 * spans,)),
+            dma((spans * pieces,)),
+            dma((spans * pieces,)),
+            dma((pieces * groups,)),
+            dma((pieces * groups,)),
+        ],
+        compiler_params=pltpu.CompilerParams(
+            collective_id=0, has_side_effects=True, vmem_limit_bytes=60 * 1024 * 1024
+        ),
+        name="pair_block",
+    )(*args)
+
+
 def local(
     experts,
     parts,
@@ -436,6 +1027,23 @@
     units, wide = expert_gate.shape[2], expert_down.shape[2]
     out_width = out_weight.shape[1]
     chips = parts // CORES
+    args = (
+        conv_value,
+        conv_gate,
+        expert_input,
+        expert_gate,
+        expert_up,
+        expert_down,
+        out_weight,
+        conv_kernel,
+        norm_gain[None, :],
+        norm_shift[None, :],
+        expert_ids.T,
+        pair_logits.T,
+        group_prob[None, :],
+    )
+    if experts == GROUPS * PAIR and chips == 2:
+        return pair_call(GROUPS, parts, args)
     edge = -(-((conv_kernel.shape[0] - 1) // 2) // 16) * 16
     anywhere = pl.BlockSpec(memory_space=pl.ANY)
     near = pl.BlockSpec(memory_space=pltpu.VMEM)
@@ -491,22 +1099,7 @@
             collective_id=0, has_side_effects=True, vmem_limit_bytes=60 * 1024 * 1024
         ),
         name="block",
-    )(
-        conv_value,
-        conv_gate,
-        expert_input,
-        expert_gate,
-        expert_up,
-        expert_down,
-        out_weight,
-        conv_kernel,
-        norm_gain[None, :],
-        norm_shift[None, :],
-        expert_ids.T,
-        pair_logits.T,
-        group_prob[None, :],
-    )
-
+    )(*args)
 
 def solution(mesh):
     placed = (

time: 58.4 us -> 45.7 us (0.78)
  the two profiles are of different devices: /device:TPU:11 before, /device:TPU:0 now
where the time goes in v1:
time: 45.7 us; the launch traced here: 45.6 us
  Pallas kernels  43.3 us (95%)
  local copies, waits for them, and re-layouts  1.67 us (4%)
  between operations  0.64 us (1%)
    pallas_call x1, Pallas kernels, pair_call(): pl.pallas_call(functools.partial(pair_kernel, groups, parts), out_shape=(...  43.3 us
    unnamed x2, local copies, waits for them, and re-layouts  1.67 us

profile of v1, /device:TPU:0, one launch (start us, length us, event | category | flops | bytes accessed | tf_op | source)
XLA Modules:
  0.0 45.6 jit_solution(4450496023335527423)
XLA Ops:
  0.6 43.3 %pair_block.1 = (bf16[512,1024]{1,0:T(8,128)(2,1)S(1)}, bf16[128,1024]{1,0:T(8,128)(2,1)S(1)}) custom-call(bf16[256,512]{1,0:T(8,128)(2,1)} %value_hbm.1, bf16[256,512]{1,0:T(8,128)(2,1)} %gate_hbm.1, bf16[128,4096]{1,0:T(8,128)(2,1)} %input_hbm.1, bf16[1,4096,512]{2,1,0:T(8,128)(2,1)} %wgate_hbm.1, bf16[1,4096,512]{2,1,0:T(8,128)(2,1)} %wup_hbm.1, ...), custom_call_target="tpu_custom_call" | custom-call | tf_op jit(solution)/shard_map/pair_block/pallas_call | solution.py:939
  43.9 1.0 %copy.17 = bf16[512,1024]{1,0:T(8,128)(2,1)} copy(bf16[512,1024]{1,0:T(8,128)(2,1)S(1)} %get-tuple-element.2) | data formatting | bytes 2097152
  44.9 0.7 %copy.18 = bf16[128,1024]{1,0:T(8,128)(2,1)} copy(bf16[128,1024]{1,0:T(8,128)(2,1)S(1)} %get-tuple-element.3) | data formatting | bytes 524288

commit v2 on v1

--- a/solution.py
+++ b/solution.py
@@ -423,20 +423,23 @@
     wup_hbm,
     wdown_hbm,
     wout_hbm,
+    taps_hbm,
+    gain_hbm,
+    shift_hbm,
+    ids_hbm,
+    logits_hbm,
+    prob_hbm,
+    mixer,
+    combined,
     taps_ref,
-    gain_ref,
-    shift_ref,
+    affine,
     ids_ref,
     logits_ref,
     prob_ref,
-    mixer,
-    combined,
-    value,
-    gate,
+    values,
     mine,
     tokens,
-    wgate,
-    wup,
+    projections,
     wdown,
     wout,
     send_rows,
@@ -456,6 +459,7 @@
     edges,
     halo,
     conv,
+    stats,
     swished,
     load_sem,
     z_send,
@@ -466,14 +470,15 @@
     y_recv,
     x_send,
     x_recv,
-    d_send,
     d_recv,
     s_send,
     s_recv,
     hal_send,
     hal_recv,
-    conv_send,
-    conv_recv,
+    stat_send,
+    stat_recv,
+    mix_send,
+    mix_recv,
     hid_send,
     hid_recv,
     res_send,
@@ -491,11 +496,10 @@
     beside = (1 - chip) * CORES + core
     opposite = (1 - chip) * CORES + 1 - core
     slots, quarter = send_rows.shape[1], send_rows.shape[2]
-    order = list(range(0, groups, 2)) + list(range(1, groups, 2))
-    spans = 2
-    per = groups // spans
-    rows = per * PAIR * slots
-    length, channels = conv.shape[1], conv.shape[2]
+    blocks = [(0, groups // 2)] + [(p, 1) for p in range(groups // 2, groups)]
+    each = PAIR * slots
+    straight = (1,)
+    length, channels = conv.shape
     edge = halo.shape[1]
     reach = (taps_ref.shape[0] - 1) // 2
 
@@ -514,28 +518,39 @@
     left, right = lax.rem(me + experts - 1, experts), lax.rem(me + 1, experts)
     barrier = pltpu.get_barrier_semaphore()
     peers = [(onward(k), tp) for k in range(1, groups)]
-    peers += [(mate, tp), (me, beside), (me, sibling), (left, tp), (right, tp)]
+    peers += [(mate, tp), (me, beside), (me, sibling), (me, opposite), (mate, beside), (left, tp), (right, tp)]
     for peer in peers:
         pl.semaphore_signal(barrier, inc=1, device_id=peer, device_id_type=MESH)
 
     columns = pl.ds(pl.multiple_of(tp * quarter, quarter), quarter)
+    def load(i, *pairs):
+        return [pltpu.make_async_copy(src, dst, load_sem.at[i]) for src, dst in pairs]
+
     loads = [
-        pltpu.make_async_copy(src, dst, load_sem.at[i])
-        for i, (src, dst) in enumerate(
-            [
-                (input_hbm.at[:, columns], mine),
-                (input_hbm, tokens),
-                (value_hbm, value),
-                (gate_hbm, gate),
-                (wgate_hbm.at[0], wgate),
-                (wup_hbm.at[0], wup),
-                (wdown_hbm.at[0], wdown),
-                (wout_hbm, wout),
-            ]
-        )
+        load(0, (ids_hbm, ids_ref)),
+        load(1, (input_hbm.at[:, columns], mine)),
+        load(2, (logits_hbm, logits_ref)),
+        load(3, (prob_hbm, prob_ref)),
+        load(4, (input_hbm, tokens)),
+        load(5, (value_hbm, values.at[0]), (gate_hbm, values.at[1])),
+        load(6, (taps_hbm, taps_ref)),
+        load(7, (wgate_hbm, projections.at[0:1]), (wup_hbm, projections.at[1:2])),
+        load(8, (wdown_hbm.at[0], wdown)),
+        load(9, (wout_hbm, wout)),
+        load(10, (gain_hbm, affine.at[0]), (shift_hbm, affine.at[1])),
     ]
-    for load in loads:
-        load.start()
+    for copies in loads:
+        for copy in copies:
+            copy.start()
+
+    def loaded(i):
+        whole = {5: values, 7: projections, 10: affine}.get(i)
+        if whole is None:
+            loads[i][0].wait()
+        else:
+            pltpu.make_async_copy(whole, whole, load_sem.at[i]).wait()
+
+    loaded(0)
 
     count = ids_ref.shape[1]
     first, second = ids_ref[0:1, :], ids_ref[1:2, :]
@@ -557,51 +572,57 @@
     def dispatch(k):
         return remote(
             send_rows.at[k - 1],
-            arrived.at[tp, order.index(k), 0],
-            z_send.at[k],
+            arrived.at[tp, k, 0],
+            z_send.at[0],
             z_recv.at[k],
             ep=onward(k),
         )
 
-    loads[0].wait()
+    loaded(1)
     picked = jnp.dot(place[slots:], mine[...], preferred_element_type=F32)
     send_rows[...] = picked.astype(BF16).reshape(groups - 1, slots, quarter)
     pl.semaphore_wait(barrier, len(peers))
-    for k in order[1:]:
+    for k in range(1, groups):
         dispatch(k).start()
 
     def to_beside(p):
         return remote(
-            arrived.at[tp, p, 0], arrived.at[tp, p, 0], y_send.at[p], y_recv.at[p], part=beside
+            arrived.at[tp, p, 0], arrived.at[tp, p, 0], y_send.at[0], y_recv.at[p], part=beside
         )
 
     def to_mate(p):
-        return remote(arrived.at[tp, p, 0], arrived.at[tp, p, 1], x_send.at[p], x_recv.at[p], ep=mate)
+        return remote(arrived.at[tp, p, 0], arrived.at[tp, p, 1], x_send.at[0], x_recv.at[p], ep=mate)
 
     def across(p):
         if p == 0:
             return remote(
-                arrived.at[beside, 0, 0], arrived.at[beside, 0, 1], d_send.at[0], d_recv.at[0], ep=mate
+                arrived.at[beside, 0, 0], arrived.at[beside, 0, 1], x_send.at[0], d_recv.at[0], ep=mate
             )
-        lead = core == 0
-        block = jnp.where(lead, tp, beside)
+        if p in straight:
+            return remote(
+                arrived.at[tp, p, 0], arrived.at[tp, p, 1], x_send.at[0], d_recv.at[p], ep=mate, part=beside
+            )
         return remote(
-            arrived.at[block, p, 1 - core],
-            arrived.at[block, p, 1],
-            d_send.at[p],
-            d_recv.at[p],
-            ep=jnp.where(lead, me, mate),
-            part=jnp.where(lead, beside, tp),
+            arrived.at[beside, p, 0], arrived.at[beside, p, 1], x_send.at[0], d_recv.at[p], ep=mate
         )
 
     def to_sibling(p, far, which):
         block = beside if far else tp
-        i = 4 * p + 2 * which + far
         return remote(
-            arrived.at[block, p, which], arrived.at[block, p, which], s_send.at[i], s_recv.at[i], part=sibling
-        )
-
-    loads[1].wait()
+            arrived.at[block, p, which],
+            arrived.at[block, p, which],
+            s_send.at[min(p, 1)],
+            s_recv.at[sum(start <= p for start, _ in blocks) - 1],
+            part=sibling,
+        )
+
+    def all_sent(whole, sem):
+        remote(whole, whole, sem, sem, part=sibling).wait_send()
+
+    def all_received(whole, sem):
+        remote(whole, whole, sem, sem, part=sibling).wait_recv()
+
+    loaded(4)
     for q in range(parts):
         picked = jnp.dot(
             place[:slots], tokens[:, q * quarter : (q + 1) * quarter], preferred_element_type=F32
@@ -610,6 +631,8 @@
     to_mate(0).start()
     across(0).start()
 
+    loaded(2)
+    loaded(3)
     share = jax.nn.sigmoid(logits_ref[0:1, :] - logits_ref[1:2, :])
     of_first = share * prob_ref[...]
     of_second = (1.0 - share) * prob_ref[...]
@@ -621,23 +644,23 @@
     weights[...] = both.reshape(weights.shape)
 
     def give_weights(k):
-        return remote(weights.at[k], arrived_weights.at[k], w_send.at[k], w_recv.at[k], ep=onward(k))
-
-    for k in order[1:]:
-        give_weights(k).start()
+        return remote(weights.at[k], arrived_weights.at[k], w_send.at[0], w_recv.at[0], ep=onward(k))
+
     arrived_weights[0] = weights[0]
     scatter[...] = jnp.transpose(place_f, (1, 0)).astype(BF16)
 
-    loads[2].wait()
-    loads[3].wait()
-    gated = (value[...].astype(F32) * jax.nn.sigmoid(gate[...].astype(F32))).astype(BF16)
+    loaded(5)
+    loaded(6)
+    gated = (values[0].astype(F32) * jax.nn.sigmoid(values[1].astype(F32))).astype(BF16)
     padded[edge : edge + length, :] = jnp.transpose(gated.astype(F32), (1, 0))
     edges[0] = padded[edge : 2 * edge, :].astype(BF16)
     edges[1] = padded[length : length + edge, :].astype(BF16)
     to_left = remote(edges.at[0], halo.at[1], hal_send.at[0], hal_recv.at[0], ep=left)
-    to_right = remote(edges.at[1], halo.at[0], hal_send.at[1], hal_recv.at[1], ep=right)
+    to_right = remote(edges.at[1], halo.at[0], hal_send.at[0], hal_recv.at[0], ep=right)
     to_left.start()
     to_right.start()
+    for k in range(1, groups):
+        give_weights(k).start()
     taps = taps_ref[...].astype(F32)
     chunk, chunks = tiles(length, 64)
 
@@ -646,277 +669,290 @@
         for j in range(taps.shape[0]):
             start = i * chunk + j + edge - reach
             total = total + taps[j : j + 1, :] * padded[start : start + chunk, :]
-        conv[tp, i * chunk : (i + 1) * chunk, :] = total.astype(BF16)
+        conv[i * chunk : (i + 1) * chunk, :] = total.astype(BF16)
 
     def landed(p):
-        dispatch(order[p]).wait_recv()
+        dispatch(p).wait_recv()
         to_beside(p).start()
         to_mate(p).start()
+        if p in straight:
+            across(p).start()
         to_sibling(p, 0, 0).start()
 
     def turned(p):
         if p:
             to_beside(p).wait_recv()
+            if p not in straight:
+                across(p).start()
+            to_sibling(p, 1, 0).start()
         to_mate(p).wait_recv()
-        if p:
-            across(p).start()
-            to_sibling(p, 1, 0).start()
         to_sibling(p, 0, 1).start()
 
     def closed(p):
         across(p).wait_recv()
         to_sibling(p, 1, 1).start()
 
-    inner = list(range(1, chunks - 1))
-    early = inner[: len(inner) // 3]
-    middle = inner[len(inner) // 3 : 2 * len(inner) // 3]
-    late = inner[2 * len(inner) // 3 :]
-    for i in early:
+    def measure():
+        block = conv[...].astype(F32)
+        center = jnp.sum(block, axis=1, keepdims=True) / channels
+        block = block - center
+        spread = jnp.sum(block * block, axis=1, keepdims=True)
+        lane = lax.broadcasted_iota(jnp.int32, (length, 128), 1)
+        turned_over = jnp.transpose(jnp.where(lane == 0, center, spread), (1, 0))
+        lanes = stats.shape[2]
+        for i in range(length // lanes):
+            span = slice(i * lanes, (i + 1) * lanes)
+            stats[tp, i : i + 1] = turned_over[0:1, span]
+            stats[tp, i + length // lanes : i + 1 + length // lanes] = turned_over[1:2, span]
+        for i in range(3):
+            tell(i).start()
+
+    def tell(i):
+        part = (sibling, beside, opposite)[i]
+        return remote(stats.at[tp], stats.at[tp], stat_send.at[0], stat_recv.at[0], part=part)
+
+    def normalize():
+        all_received(stats.at[0:3], stat_recv.at[0])
+        wraps = length // stats.shape[2]
+        centers = [stats[b, 0:wraps] for b in range(parts)]
+        center = sum(centers) / parts
+        spread = sum(
+            stats[b, wraps : 2 * wraps] + channels * jnp.square(centers[b] - center) for b in range(parts)
+        )
+        scale = lax.rsqrt(spread / (parts * channels) + 1e-05)
+        row = lax.broadcasted_iota(jnp.int32, (128, stats.shape[2]), 0)
+        turned_over = [
+            jnp.transpose(jnp.where(row == 0, center[i : i + 1], scale[i : i + 1]), (1, 0)) for i in range(wraps)
+        ]
+        across_rows = jnp.concatenate(turned_over, axis=0)
+        center, scale = across_rows[:, 0:1], across_rows[:, 1:2]
+        lanes = pl.ds(pl.multiple_of(tp * channels, channels), channels)
+        normed = (conv[...].astype(F32) - center) * scale * affine[0, :, lanes] + affine[1, :, lanes]
+        swished[tp] = jax.nn.silu(normed).astype(BF16)
+
+    cuts = mix_recv.shape[0] // 2
+    share_rows = length // cuts
+
+    def share_copy(i, kind):
+        cut = pl.ds(i * share_rows, share_rows)
+        block = beside if kind == 2 else tp
+        j = 2 * cuts if kind == 1 else 2 * i + kind // 2
+        return remote(
+            swished.at[block, cut],
+            swished.at[block, cut],
+            mix_send.at[0],
+            mix_recv.at[j],
+            part=beside if kind == 0 else sibling,
+        )
+
+    units = hidden.shape[2]
+    tile, steps = tiles(units, 256)
+
+    def extent(h):
+        start, size = blocks[h]
+        return slice(start * each, (start + size) * each)
+
+    def deep(q):
+        return pl.ds(pl.multiple_of(q * quarter, quarter), quarter)
+
+    def project(h, quarters, begin):
+        start, size = blocks[h]
+        for i in range(steps):
+            span = slice(i * tile, (i + 1) * tile)
+            for which, total in enumerate((gate_sum, up_sum)):
+                product = sum(
+                    jnp.dot(
+                        arrived[q, start : start + size].reshape(size * each, quarter),
+                        projections[which, deep(q), span],
+                        preferred_element_type=F32,
+                    )
+                    for q in quarters
+                )
+                total[extent(h), span] = product if begin else total[extent(h), span] + product
+
+    def hid_copy(h, kind):
+        block = beside if kind == 2 else tp
+        j = 3 * h + kind
+        return remote(
+            hidden.at[block, extent(h)],
+            hidden.at[block, extent(h)],
+            hid_send.at[0],
+            hid_recv.at[j],
+            part=beside if kind == 0 else sibling,
+        )
+
+    def near(h):
+        project(h, (tp, beside), True)
+
+    def far(h):
+        start, size = blocks[h]
+        whole = arrived.at[0:2, start : start + size] if start else arrived.at[0 : 2 * size - 1, 0]
+        all_received(whole, s_recv.at[h])
+        project(h, (sibling, opposite), False)
+        hidden[tp, extent(h)] = (jax.nn.silu(gate_sum[extent(h)]) * up_sum[extent(h)]).astype(BF16)
+        hid_copy(h, 0).start()
+        hid_copy(h, 1).start()
+
+    wide = down_sum.shape[1]
+    pieces = result.shape[0]
+    span_wide = wide // pieces
+    cols = [slice(c * span_wide, (c + 1) * span_wide) for c in range(pieces)]
+
+    def down(h, block, c):
+        depth = pl.ds(pl.multiple_of(block * units, units), units)
+        return jnp.dot(hidden[block, extent(h)], wdown[depth, cols[c]], preferred_element_type=F32)
+
+    def down_near(h):
+        hid_copy(h, 1).wait_recv()
+        for c in range(pieces):
+            down_sum[extent(h), cols[c]] = down(h, tp, c) + down(h, sibling, c)
+
+    def hand_on(h):
+        hid_copy(h, 0).wait_recv()
+        hid_copy(h, 2).start()
+
+    def exchange(h, c):
+        start, size = blocks[h]
+        return remote(
+            result.at[c, 1, start : start + size],
+            other_result.at[c, start : start + size],
+            res_send.at[0],
+            res_recv.at[pieces * h + c],
+            ep=mate,
+        )
+
+    def down_far(h):
+        start, size = blocks[h]
+        for c in range(pieces):
+            down_sum[extent(h), cols[c]] += down(h, beside, c)
+        hid_copy(h, 2).wait_recv()
+        for c in range(pieces):
+            total = (down_sum[extent(h), cols[c]] + down(h, opposite, c)).astype(BF16)
+            total = total.reshape(size, PAIR, slots, span_wide)
+            for which in range(PAIR):
+                result[c, which, start : start + size] = total[:, which]
+            exchange(h, c).start()
+
+    def give_back(k, c):
+        return remote(summed.at[c, k], returned.at[c, k], ret_send.at[0], ret_recv.at[c], ep=backward(k))
+
+    def combine(h, c):
+        if h == 0 and c == 0:
+            all_received(arrived_weights.at[1:groups], w_recv.at[0])
+        exchange(h, c).wait_recv()
+        start, size = blocks[h]
+        for k in range(start, start + size):
+            middle = weights.shape[2] // 2
+            ours = arrived_weights[k, :, 0:1]
+            theirs = arrived_weights[k, :, middle : middle + 1]
+            total = ours * result[c, 0, k].astype(F32) + theirs * other_result[c, k].astype(F32)
+            if k:
+                summed[c, k] = total.astype(BF16)
+                give_back(k, c).start()
+            else:
+                returned[c, 0] = total.astype(BF16)
+
+    out_tile, out_steps = tiles(mixer.shape[1], 256)
+
+    def mix(cut):
+        cut_rows = pl.ds(cut * share_rows, share_rows)
+
+        for i in range(out_steps):
+            span = slice(i * out_tile, (i + 1) * out_tile)
+            total = sum(
+                jnp.dot(swished[b, cut_rows], wout[b * channels : (b + 1) * channels, span], preferred_element_type=F32)
+                for b in range(parts)
+            )
+            mixer[cut_rows, span] = total.astype(BF16)
+
+    def passed(i):
+        share_copy(i, 0).wait_recv()
+        share_copy(i, 2).start()
+
+    def mixed(i):
+        if i == 0:
+            all_received(swished.at[0], mix_recv.at[2 * cuts])
+        share_copy(i, 2).wait_recv()
+        mix(i)
+
+    def combined_block(h):
+        for c in range(pieces):
+            combine(h, c)
+
+    for i in range(1, chunks - 1):
         convolve(i)
     landed(1)
     turned(0)
-    for i in middle:
-        convolve(i)
     closed(0)
-    for p in range(2, groups):
-        landed(p)
-    for i in late:
-        convolve(i)
+    landed(2)
+    landed(3)
     turned(1)
-    to_left.wait()
-    to_right.wait()
+    all_received(halo, hal_recv.at[0])
     padded[0:edge, :] = jnp.where(me == 0, 0.0, halo[0].astype(F32))
     padded[edge + length : 2 * edge + length, :] = jnp.where(
         me == experts - 1, 0.0, halo[1].astype(F32)
     )
     convolve(0)
+    convolve(chunks - 1)
+    measure()
+    closed(1)
+    loaded(7)
+    near(0)
     turned(2)
-    convolve(chunks - 1)
-    for p in range(3, groups):
-        turned(p)
-
-    cuts = 2
-    share_rows = length // cuts
-
-    def conv_copy(i, kind):
-        cut = pl.ds(i * share_rows, share_rows)
-        block = beside if kind == 2 else tp
-        j = 3 * i + kind
-        return remote(
-            conv.at[block, cut],
-            conv.at[block, cut],
-            conv_send.at[j],
-            conv_recv.at[j],
-            part=beside if kind == 0 else sibling,
-        )
-
+    far(0)
+    turned(3)
+    loaded(8)
+    down_near(0)
+    loaded(10)
+    normalize()
     for i in range(cuts):
-        conv_copy(i, 1).start()
-    for p in range(1, per):
-        closed(p)
-
-    units = hidden.shape[3]
-    tile, steps = tiles(units, 256)
-
-    def gather_rows(q, h):
-        return arrived[q, h * per : (h + 1) * per].reshape(rows, quarter)
-
-    def deep(q):
-        return pl.ds(pl.multiple_of(q * quarter, quarter), quarter)
-
-    def project(h, blocks, begin):
-        for i in range(steps):
-            span = slice(i * tile, (i + 1) * tile)
-            for weight, total in ((wgate, gate_sum), (wup, up_sum)):
-                value = sum(
-                    jnp.dot(gather_rows(q, h), weight[deep(q), span], preferred_element_type=F32)
-                    for q in blocks
-                )
-                total[:, span] = value if begin else total[:, span] + value
-
-    def hid_copy(h, kind):
-        block = beside if kind == 2 else tp
-        j = 3 * h + kind
-        return remote(
-            hidden.at[h, block],
-            hidden.at[h, block],
-            hid_send.at[j],
-            hid_recv.at[j],
-            part=beside if kind == 0 else sibling,
-        )
-
-    def activate(h):
-        hidden[h, tp] = (jax.nn.silu(gate_sum[...]) * up_sum[...]).astype(BF16)
-        hid_copy(h, 0).start()
-        hid_copy(h, 1).start()
-
-    def from_sibling(h):
-        for p in range(h * per, (h + 1) * per):
-            for which in range(2):
-                for far in range(2):
-                    if p or which:
-                        to_sibling(p, far, which).wait_recv()
-
-    loads[4].wait()
-    loads[5].wait()
-    project(0, (tp, beside), True)
-    for p in range(per, groups - 1):
-        closed(p)
-    from_sibling(0)
-    project(0, (sibling, opposite), False)
-    activate(0)
-    closed(groups - 1)
-    project(1, (tp, beside), True)
-    from_sibling(1)
-    project(1, (sibling, opposite), False)
-    activate(1)
+        share_copy(i, 1).start()
+    closed(2)
+    near(1)
+    far(1)
+    closed(3)
+    near(2)
+    hand_on(0)
+    far(2)
     for i in range(cuts):
-        conv_copy(i, 0).start()
-
-    loads[6].wait()
-    wide = down_sum.shape[2]
-    pieces = result.shape[1]
-    span_wide = wide // pieces
-
-    def down(h, block, span):
-        depth = pl.ds(pl.multiple_of(block * units, units), units)
-        return jnp.dot(hidden[h, block], wdown[depth, span], preferred_element_type=F32)
-
-    def down_near(h):
-        hid_copy(h, 1).wait_recv()
-        for c in range(pieces):
-            span = slice(c * span_wide, (c + 1) * span_wide)
-            down_sum[h, :, span] = down(h, tp, span) + down(h, sibling, span)
-
-    def exchange(h, c):
-        return remote(
-            result.at[h, c, 1], other_result.at[h, c], res_send.at[2 * h + c], res_recv.at[2 * h + c], ep=mate
-        )
-
-    def down_far(h):
-        hid_copy(h, 0).wait_recv()
-        hid_copy(h, 2).start()
-        for c in range(pieces):
-            span = slice(c * span_wide, (c + 1) * span_wide)
-            total = down_sum[h, :, span] + down(h, beside, span)
-            if c == 0:
-                hid_copy(h, 2).wait_recv()
-            total = (total + down(h, opposite, span)).astype(BF16).reshape(per, PAIR, slots, span_wide)
-            for which in range(PAIR):
-                result[h, c, which] = total[:, which]
-            exchange(h, c).start()
-
-    def give_back(k, c):
-        p = order.index(k)
-        return remote(
-            summed.at[p // per, c, p % per],
-            returned.at[c, k],
-            ret_send.at[c * groups + k],
-            ret_recv.at[c * groups + k],
-            ep=backward(k),
-        )
-
-    def combine(h, c):
-        exchange(h, c).wait_recv()
-        for i in range(per):
-            k = order[h * per + i]
-            if k and c == 0:
-                give_weights(k).wait_recv()
-            half = weights.shape[2] // 2
-            ours = arrived_weights[k, :, 0:1]
-            theirs = arrived_weights[k, :, half : half + 1]
-            total = ours * result[h, c, 0, i].astype(F32) + theirs * other_result[h, c, i].astype(F32)
-            if k:
-                summed[h, c, i] = total.astype(BF16)
-                give_back(k, c).start()
-            else:
-                returned[c, 0] = total.astype(BF16)
-
-    width = parts * channels
-    norm_chunk, norm_chunks = tiles(share_rows, 64)
-
-    def normalize(cut):
-        @pl.loop(0, norm_chunks)
-        def _(i):
-            span = pl.ds(pl.multiple_of(cut * share_rows + i * norm_chunk, norm_chunk), norm_chunk)
-            blocks = [conv[b, span, :].astype(F32) for b in range(parts)]
-            center = sum(jnp.sum(block, axis=1, keepdims=True) for block in blocks) / width
-            blocks = [block - center for block in blocks]
-            spread = sum(jnp.sum(block * block, axis=1, keepdims=True) for block in blocks) / width
-            scale = lax.rsqrt(spread + 1e-05)
-            for b in range(parts):
-                lanes = slice(b * channels, (b + 1) * channels)
-                normed = blocks[b] * scale * gain_ref[:, lanes] + shift_ref[:, lanes]
-                swished[b, span, :] = jax.nn.silu(normed).astype(BF16)
-
-    out_tile, out_steps = tiles(mixer.shape[1], 256)
-
-    def mix(cut):
-        cut_rows = pl.ds(cut * share_rows, share_rows)
-
-        @pl.loop(0, out_steps)
-        def _(i):
-            span = pl.ds(pl.multiple_of(i * out_tile, out_tile), out_tile)
-            total = jnp.zeros((share_rows, out_tile), F32)
-            for b in range(parts):
-                total = total + jnp.dot(
-                    swished[b, cut_rows], wout[b * channels : (b + 1) * channels, span], preferred_element_type=F32
-                )
-            mixer[cut_rows, span] = total.astype(BF16)
-
-    down_near(0)
+        share_copy(i, 0).start()
     down_far(0)
     down_near(1)
+    hand_on(1)
+    down_near(2)
     down_far(1)
+    hand_on(2)
+    combine(0, 0)
+    down_far(2)
+    for c in range(1, pieces):
+        combine(0, c)
+    combined_block(1)
+    passed(0)
+    combined_block(2)
+    loaded(9)
+    mixed(0)
+    for i in range(1, cuts):
+        passed(i)
+        mixed(i)
     for c in range(pieces):
-        combine(0, c)
-    for i in range(cuts):
-        conv_copy(i, 1).wait_recv()
-    conv_copy(0, 0).wait_recv()
-    conv_copy(0, 2).start()
-    for c in range(pieces):
-        combine(1, c)
-    loads[7].wait()
-    conv_copy(0, 2).wait_recv()
-    normalize(0)
-    mix(0)
-    for i in range(1, cuts):
-        conv_copy(i, 0).wait_recv()
-        conv_copy(i, 2).start()
-    for i in range(1, cuts):
-        conv_copy(i, 2).wait_recv()
-        normalize(i)
-        mix(i)
-    for c in range(pieces):
-        for k in range(1, groups):
-            give_back(k, c).wait_recv()
+        all_received(returned.at[c, 1:groups], ret_recv.at[c])
         block = returned[c].reshape(groups * slots, span_wide)
         combined[:, c * span_wide : (c + 1) * span_wide] = jnp.dot(
             scatter[...], block, preferred_element_type=F32
         ).astype(BF16)
 
-    for k in range(1, groups):
-        dispatch(k).wait_send()
-        give_weights(k).wait_send()
-        for c in range(pieces):
-            give_back(k, c).wait_send()
-    for p in range(groups):
-        if p:
-            to_beside(p).wait_send()
-        to_mate(p).wait_send()
-        across(p).wait_send()
-        for which in range(2):
-            for far in range(2):
-                if p or which:
-                    to_sibling(p, far, which).wait_send()
-    for kind in range(3):
-        for i in range(cuts):
-            conv_copy(i, kind).wait_send()
-        for h in range(spans):
-            hid_copy(h, kind).wait_send()
-    for h in range(spans):
-        for c in range(pieces):
-            exchange(h, c).wait_send()
+    all_sent(send_rows, z_send.at[0])
+    all_sent(weights.at[1:groups], w_send.at[0])
+    all_sent(arrived.at[0, 1:groups, 0], y_send.at[0])
+    all_sent(arrived.at[0], x_send.at[0])
+    all_sent(arrived.at[0, 0], s_send.at[0])
+    all_sent(arrived.at[0:2, 1:groups], s_send.at[1])
+    all_sent(edges, hal_send.at[0])
+    all_sent(stats.at[0:3], stat_send.at[0])
+    all_sent(swished.at[0:3], mix_send.at[0])
+    all_sent(hidden.at[0:3], hid_send.at[0])
+    all_sent(other_result, res_send.at[0])
+    all_sent(summed.at[:, 1:groups], ret_send.at[0])
 
 
 def pair_call(groups, parts, args):
@@ -929,9 +965,8 @@
     units, wide = expert_gate.shape[2], expert_down.shape[2]
     out_width = out_weight.shape[1]
     edge = -(-((conv_kernel.shape[0] - 1) // 2) // 16) * 16
-    spans, cuts, pieces = 2, 2, 2
-    per = groups // spans
-    rows = per * PAIR * slots
+    cuts, pieces, blocks = 2, 2, groups // 2 + 1
+    rows = groups * PAIR * slots
     piece = wide // pieces
     anywhere = pl.BlockSpec(memory_space=pl.ANY)
     near = pl.BlockSpec(memory_space=pltpu.VMEM)
@@ -942,15 +977,16 @@
             pltpu.VMEM((length, out_width), BF16),
             pltpu.VMEM((count, wide), BF16),
         ),
-        in_specs=[anywhere] * 7 + [near] * 6,
+        in_specs=[anywhere] * 13,
         out_specs=(near, near),
         scratch_shapes=[
-            pltpu.VMEM((channels, length), BF16),
-            pltpu.VMEM((channels, length), BF16),
+            pltpu.VMEM(args[7].shape, args[7].dtype),
+            pltpu.VMEM((2, *args[8].shape), F32),
+            *[pltpu.VMEM(arg.shape, arg.dtype) for arg in args[10:]],
+            pltpu.VMEM((2, channels, length), BF16),
             pltpu.VMEM((count, quarter), BF16),
             pltpu.VMEM((count, model), BF16),
-            pltpu.VMEM((model, units), BF16),
-            pltpu.VMEM((model, units), BF16),
+            pltpu.VMEM((2, model, units), BF16),
             pltpu.VMEM(expert_down.shape[1:], BF16),
             pltpu.VMEM(out_weight.shape, BF16),
             pltpu.VMEM((groups - 1, slots, quarter), BF16),
@@ -959,41 +995,43 @@
             pltpu.VMEM((parts, groups, PAIR, slots, quarter), BF16),
             pltpu.VMEM((rows, units), F32),
             pltpu.VMEM((rows, units), F32),
-            pltpu.VMEM((spans, parts, rows, units), BF16),
-            pltpu.VMEM((spans, rows, wide), F32),
-            pltpu.VMEM((spans, pieces, PAIR, per, slots, piece), BF16),
-            pltpu.VMEM((spans, pieces, per, slots, piece), BF16),
-            pltpu.VMEM((spans, pieces, per, slots, piece), BF16),
+            pltpu.VMEM((parts, rows, units), BF16),
+            pltpu.VMEM((rows, wide), F32),
+            pltpu.VMEM((pieces, PAIR, groups, slots, piece), BF16),
+            pltpu.VMEM((pieces, groups, slots, piece), BF16),
+            pltpu.VMEM((pieces, groups, slots, piece), BF16),
             pltpu.VMEM((pieces, groups, slots, piece), BF16),
             pltpu.VMEM((count, groups * slots), BF16),
             pltpu.VMEM((length + 2 * edge, channels), F32),
             pltpu.VMEM((2, edge, channels), BF16),
             pltpu.VMEM((2, edge, channels), BF16),
+            pltpu.VMEM((length, channels), BF16),
+            pltpu.VMEM((parts, 2 * length // 128, 128), F32),
             pltpu.VMEM((parts, length, channels), BF16),
-            pltpu.VMEM((parts, length, channels), BF16),
-            dma((8,)),
+            dma((11,)),
+            dma((1,)),
+            dma((groups,)),
+            dma((1,)),
+            dma((1,)),
+            dma((1,)),
+            dma((groups,)),
+            dma((1,)),
             dma((groups,)),
             dma((groups,)),
-            dma((groups,)),
-            dma((groups,)),
-            dma((groups,)),
-            dma((groups,)),
-            dma((groups,)),
-            dma((groups,)),
-            dma((groups,)),
-            dma((groups,)),
-            dma((4 * groups,)),
-            dma((4 * groups,)),
             dma((2,)),
-            dma((2,)),
-            dma((3 * cuts,)),
-            dma((3 * cuts,)),
-            dma((3 * spans,)),
-            dma((3 * spans,)),
-            dma((spans * pieces,)),
-            dma((spans * pieces,)),
-            dma((pieces * groups,)),
-            dma((pieces * groups,)),
+            dma((blocks,)),
+            dma((1,)),
+            dma((1,)),
+            dma((1,)),
+            dma((1,)),
+            dma((1,)),
+            dma((2 * cuts + 1,)),
+            dma((1,)),
+            dma((3 * blocks,)),
+            dma((1,)),
+            dma((blocks * pieces,)),
+            dma((1,)),
+            dma((pieces,)),
         ],
         compiler_params=pltpu.CompilerParams(
             collective_id=0, has_side_effects=True, vmem_limit_bytes=60 * 1024 * 1024

time: 45.7 us -> 40.5 us (0.89)
  Pallas kernels: 43.3 us -> 38.1 us
    pallas_call x1, Pallas kernels: 43.3 us -> 38.1 us  [pair_call(): pl.pallas_call(functools.partial(pair_kernel, groups, parts), out_shape=(...]
where the time goes in v2:
time: 40.5 us; the launch traced here: 40.4 us
  Pallas kernels  38.1 us (94%)
  local copies, waits for them, and re-layouts  1.67 us (4%)
  between operations  0.64 us (2%)
    pallas_call x1, Pallas kernels, pair_call(): pl.pallas_call(functools.partial(pair_kernel, groups, parts), out_shape=(...  38.1 us
    unnamed x2, local copies, waits for them, and re-layouts  1.67 us

profile of v2, /device:TPU:0, one launch (start us, length us, event | category | flops | bytes accessed | tf_op | source)
XLA Modules:
  0.0 40.4 jit_solution(1275139480115429364)
XLA Ops:
  0.6 38.1 %pair_block.1 = (bf16[512,1024]{1,0:T(8,128)(2,1)S(1)}, bf16[128,1024]{1,0:T(8,128)(2,1)S(1)}) custom-call(bf16[256,512]{1,0:T(8,128)(2,1)} %value_hbm.1, bf16[256,512]{1,0:T(8,128)(2,1)} %gate_hbm.1, bf16[128,4096]{1,0:T(8,128)(2,1)} %input_hbm.1, bf16[1,4096,512]{2,1,0:T(8,128)(2,1)} %wgate_hbm.1, bf16[1,4096,512]{2,1,0:T(8,128)(2,1)} %wup_hbm.1, ...), custom_call_target="tpu_custom_call" | custom-call | tf_op jit(solution)/shard_map/pair_block/pallas_call | solution.py:974
  38.7 1.0 %copy.17 = bf16[512,1024]{1,0:T(8,128)(2,1)} copy(bf16[512,1024]{1,0:T(8,128)(2,1)S(1)} %get-tuple-element.2) | data formatting | bytes 2097152
  39.7 0.7 %copy.18 = bf16[128,1024]{1,0:T(8,128)(2,1)} copy(bf16[128,1024]{1,0:T(8,128)(2,1)S(1)} %get-tuple-element.3) | data formatting | bytes 524288

commit v3 on v2

--- a/solution.py
+++ b/solution.py
@@ -430,7 +430,8 @@
     logits_hbm,
     prob_hbm,
     mixer,
-    combined,
+    returned,
+    scatter,
     taps_ref,
     affine,
     ids_ref,
@@ -453,8 +454,6 @@
     result,
     other_result,
     summed,
-    returned,
-    scatter,
     padded,
     edges,
     halo,
@@ -510,10 +509,10 @@
         )
 
     def onward(k):
-        return lax.rem(group + k, groups) * PAIR + side
+        return jnp.bitwise_xor(group, k) * PAIR + side
 
     def backward(k):
-        return lax.rem(group + groups - k, groups) * PAIR + side
+        return jnp.bitwise_xor(group, k) * PAIR + side
 
     left, right = lax.rem(me + experts - 1, experts), lax.rem(me + 1, experts)
     barrier = pltpu.get_barrier_semaphore()
@@ -554,8 +553,7 @@
 
     count = ids_ref.shape[1]
     first, second = ids_ref[0:1, :], ids_ref[1:2, :]
-    position = lax.broadcasted_iota(jnp.int32, (groups, count), 0) + group
-    position = jnp.where(position >= groups, position - groups, position) * PAIR
+    position = jnp.bitwise_xor(lax.broadcasted_iota(jnp.int32, (groups, count), 0), group) * PAIR
     chosen = jnp.where((first >= position) & (first < position + PAIR), 1.0, 0.0).astype(F32)
     earlier = lax.broadcasted_iota(jnp.int32, (count, count), 0) < lax.broadcasted_iota(
         jnp.int32, (count, count), 1
@@ -680,11 +678,12 @@
         to_sibling(p, 0, 0).start()
 
     def turned(p):
-        if p:
-            to_beside(p).wait_recv()
-            if p not in straight:
-                across(p).start()
-            to_sibling(p, 1, 0).start()
+        to_beside(p).wait_recv()
+        if p not in straight:
+            across(p).start()
+        to_sibling(p, 1, 0).start()
+
+    def met(p):
         to_mate(p).wait_recv()
         to_sibling(p, 0, 1).start()
 
@@ -782,7 +781,10 @@
         )
 
     def near(h):
-        project(h, (tp, beside), True)
+        project(h, (tp,), True)
+
+    def next_near(h):
+        project(h, (beside,), False)
 
     def far(h):
         start, size = blocks[h]
@@ -811,13 +813,12 @@
         hid_copy(h, 0).wait_recv()
         hid_copy(h, 2).start()
 
-    def exchange(h, c):
-        start, size = blocks[h]
+    def exchange(p, c):
         return remote(
-            result.at[c, 1, start : start + size],
-            other_result.at[c, start : start + size],
+            result.at[c, 1, p],
+            other_result.at[c, p],
             res_send.at[0],
-            res_recv.at[pieces * h + c],
+            res_recv.at[pieces * p + c],
             ep=mate,
         )
 
@@ -831,20 +832,18 @@
             total = total.reshape(size, PAIR, slots, span_wide)
             for which in range(PAIR):
                 result[c, which, start : start + size] = total[:, which]
-            exchange(h, c).start()
+            for p in range(max(start, 1), start + size):
+                exchange(p, c).start()
 
     def give_back(k, c):
         return remote(summed.at[c, k], returned.at[c, k], ret_send.at[0], ret_recv.at[c], ep=backward(k))
 
-    def combine(h, c):
-        if h == 0 and c == 0:
-            all_received(arrived_weights.at[1:groups], w_recv.at[0])
-        exchange(h, c).wait_recv()
-        start, size = blocks[h]
-        for k in range(start, start + size):
-            middle = weights.shape[2] // 2
-            ours = arrived_weights[k, :, 0:1]
-            theirs = arrived_weights[k, :, middle : middle + 1]
+    def combine(k):
+        middle = weights.shape[2] // 2
+        ours = arrived_weights[k, :, 0:1]
+        theirs = arrived_weights[k, :, middle : middle + 1]
+        for c in range(pieces):
+            exchange(k, c).wait_recv()
             total = ours * result[c, 0, k].astype(F32) + theirs * other_result[c, k].astype(F32)
             if k:
                 summed[c, k] = total.astype(BF16)
@@ -875,18 +874,17 @@
         share_copy(i, 2).wait_recv()
         mix(i)
 
-    def combined_block(h):
-        for c in range(pieces):
-            combine(h, c)
-
     for i in range(1, chunks - 1):
         convolve(i)
     landed(1)
-    turned(0)
+    met(0)
     closed(0)
     landed(2)
     landed(3)
     turned(1)
+    met(1)
+    loaded(7)
+    near(0)
     all_received(halo, hal_recv.at[0])
     padded[0:edge, :] = jnp.where(me == 0, 0.0, halo[0].astype(F32))
     padded[edge + length : 2 * edge + length, :] = jnp.where(
@@ -896,11 +894,14 @@
     convolve(chunks - 1)
     measure()
     closed(1)
-    loaded(7)
-    near(0)
+    next_near(0)
     turned(2)
     far(0)
     turned(3)
+    met(2)
+    near(1)
+    met(3)
+    near(2)
     loaded(8)
     down_near(0)
     loaded(10)
@@ -908,10 +909,10 @@
     for i in range(cuts):
         share_copy(i, 1).start()
     closed(2)
-    near(1)
+    next_near(1)
     far(1)
     closed(3)
-    near(2)
+    next_near(2)
     hand_on(0)
     far(2)
     for i in range(cuts):
@@ -922,25 +923,22 @@
     down_near(2)
     down_far(1)
     hand_on(2)
-    combine(0, 0)
+    all_received(arrived_weights.at[1:groups], w_recv.at[0])
     down_far(2)
-    for c in range(1, pieces):
-        combine(0, c)
-    combined_block(1)
+    for c in range(pieces):
+        exchange(0, c).start()
+    combine(1)
+    combine(2)
     passed(0)
-    combined_block(2)
+    combine(3)
     loaded(9)
     mixed(0)
+    combine(0)
     for i in range(1, cuts):
         passed(i)
         mixed(i)
     for c in range(pieces):
         all_received(returned.at[c, 1:groups], ret_recv.at[c])
-        block = returned[c].reshape(groups * slots, span_wide)
-        combined[:, c * span_wide : (c + 1) * span_wide] = jnp.dot(
-            scatter[...], block, preferred_element_type=F32
-        ).astype(BF16)
-
     all_sent(send_rows, z_send.at[0])
     all_sent(weights.at[1:groups], w_send.at[0])
     all_sent(arrived.at[0, 1:groups, 0], y_send.at[0])
@@ -953,6 +951,20 @@
     all_sent(hidden.at[0:3], hid_send.at[0])
     all_sent(other_result, res_send.at[0])
     all_sent(summed.at[:, 1:groups], ret_send.at[0])
+
+
+def store(mixer, returned, scatter, mixer_hbm, combined_hbm, combined, sem):
+    put_mixer = pltpu.make_async_copy(mixer, mixer_hbm, sem.at[0])
+    put_mixer.start()
+    pieces, groups, slots, piece = returned.shape
+    for c in range(pieces):
+        combined[:, c * piece : (c + 1) * piece] = jnp.dot(
+            scatter[...], returned[c].reshape(groups * slots, piece), preferred_element_type=F32
+        ).astype(BF16)
+    put_combined = pltpu.make_async_copy(combined, combined_hbm, sem.at[1])
+    put_combined.start()
+    put_mixer.wait()
+    put_combined.wait()
 
 
 def pair_call(groups, parts, args):
@@ -971,14 +983,15 @@
     anywhere = pl.BlockSpec(memory_space=pl.ANY)
     near = pl.BlockSpec(memory_space=pltpu.VMEM)
     dma = pltpu.SemaphoreType.DMA
-    return pl.pallas_call(
+    results = pl.pallas_call(
         functools.partial(pair_kernel, groups, parts),
         out_shape=(
             pltpu.VMEM((length, out_width), BF16),
-            pltpu.VMEM((count, wide), BF16),
+            pltpu.VMEM((pieces, groups, slots, piece), BF16),
+            pltpu.VMEM((count, groups * slots), BF16),
         ),
         in_specs=[anywhere] * 13,
-        out_specs=(near, near),
+        out_specs=(near, near, near),
         scratch_shapes=[
             pltpu.VMEM(args[7].shape, args[7].dtype),
             pltpu.VMEM((2, *args[8].shape), F32),
@@ -1000,8 +1013,6 @@
             pltpu.VMEM((pieces, PAIR, groups, slots, piece), BF16),
             pltpu.VMEM((pieces, groups, slots, piece), BF16),
             pltpu.VMEM((pieces, groups, slots, piece), BF16),
-            pltpu.VMEM((pieces, groups, slots, piece), BF16),
-            pltpu.VMEM((count, groups * slots), BF16),
             pltpu.VMEM((length + 2 * edge, channels), F32),
             pltpu.VMEM((2, edge, channels), BF16),
             pltpu.VMEM((2, edge, channels), BF16),
@@ -1029,7 +1040,7 @@
             dma((1,)),
             dma((3 * blocks,)),
             dma((1,)),
-            dma((blocks * pieces,)),
+            dma((groups * pieces,)),
             dma((1,)),
             dma((pieces,)),
         ],
@@ -1038,6 +1049,18 @@
         ),
         name="pair_block",
     )(*args)
+    results = [pltpu.with_memory_space_constraint(value, pltpu.VMEM) for value in results]
+    return pl.pallas_call(
+        store,
+        out_shape=(
+            jax.ShapeDtypeStruct((length, out_width), BF16),
+            jax.ShapeDtypeStruct((count, wide), BF16),
+        ),
+        in_specs=[near] * 3,
+        out_specs=(pl.BlockSpec(memory_space=pltpu.HBM),) * 2,
+        scratch_shapes=[pltpu.VMEM((count, wide), BF16), dma((2,))],
+        name="store",
+    )(*results)
 
 
 def local(

time: 40.5 us -> 38 us (0.938)
  local copies, waits for them, and re-layouts: 1.67 us -> 0 us
  Pallas kernels: 38.1 us -> 37.2 us
    pallas_call x1, Pallas kernels: 38.1 us -> 36.2 us  [pair_call(): pl.pallas_call(functools.partial(pair_kernel, groups, parts), out_shape=(...]
    unnamed x2 -> x0, local copies, waits for them, and re-layouts: 1.67 us -> none
    pallas_call x0 -> x1, Pallas kernels: none -> 1.08 us  [pair_call(): pl.pallas_call(store, out_shape=(jax.ShapeDtypeStruct((length, out_width)...]
where the time goes in v3:
time: 38 us; the launch traced here: 37.9 us
  Pallas kernels  37.2 us (98%)
  between operations  0.64 us (2%)
    pallas_call x1, Pallas kernels, pair_call(): pl.pallas_call(functools.partial(pair_kernel, groups, parts), out_shape=(...  36.2 us
    pallas_call x1, Pallas kernels, pair_call(): pl.pallas_call(store, out_shape=(jax.ShapeDtypeStruct((length, out_width)...  1.08 us

profile of v3, /device:TPU:0, one launch (start us, length us, event | category | flops | bytes accessed | tf_op | source)
XLA Modules:
  0.0 37.9 jit_solution(3827526393528036290)
XLA Ops:
  0.6 36.2 %pair_block.1 = (bf16[512,1024]{1,0:T(8,128)(2,1)S(1)}, bf16[2,4,32,512]{3,2,1,0:T(8,128)(2,1)S(1)}, bf16[128,128]{1,0:T(8,128)(2,1)S(1)}) custom-call(bf16[256,512]{1,0:T(8,128)(2,1)} %value_hbm.1, bf16[256,512]{1,0:T(8,128)(2,1)} %gate_hbm.1, bf16[128,4096]{1,0:T(8,128)(2,1)} %input_hbm.1, bf16[1,4096,512]{2,1,0:T(8,128)(2,1)} %wgate_hbm.1, ...), custom_call_target="tpu_custom_call" | custom-call | tf_op jit(solution)/shard_map/pair_block/pallas_call | solution.py:986
  36.8 1.1 %store.1 = (bf16[512,1024]{1,0:T(8,128)(2,1)}, bf16[128,1024]{1,0:T(8,128)(2,1)}) custom-call(bf16[512,1024]{1,0:T(8,128)(2,1)S(1)} %get-tuple-element.5.mixer, bf16[2,4,32,512]{3,2,1,0:T(8,128)(2,1)S(1)} %get-tuple-element.6.returned, bf16[128,128]{1,0:T(8,128)(2,1)S(1)} %get-tuple-element.7.scatter), custom_call_target="tpu_custom_call" | custom-call | tf_op jit(solution)/shard_map/store/pallas_call | solution.py:1053

commit v4 on v3

--- a/solution.py
+++ b/solution.py
@@ -610,7 +610,7 @@
             arrived.at[block, p, which],
             arrived.at[block, p, which],
             s_send.at[min(p, 1)],
-            s_recv.at[sum(start <= p for start, _ in blocks) - 1],
+            s_recv.at[2 * sum(start <= p for start, _ in blocks) - 2 + far],
             part=sibling,
         )
 
@@ -786,14 +786,20 @@
     def next_near(h):
         project(h, (beside,), False)
 
-    def far(h):
+    def from_sibling(h, beyond):
         start, size = blocks[h]
-        whole = arrived.at[0:2, start : start + size] if start else arrived.at[0 : 2 * size - 1, 0]
-        all_received(whole, s_recv.at[h])
-        project(h, (sibling, opposite), False)
+        whole = arrived.at[0, start : start + size] if start else arrived.at[0 : 2 * size - 1, 0, 0]
+        all_received(whole, s_recv.at[2 * h + beyond])
+        project(h, (opposite if beyond else sibling,), False)
+
+    def activate(h):
         hidden[tp, extent(h)] = (jax.nn.silu(gate_sum[extent(h)]) * up_sum[extent(h)]).astype(BF16)
         hid_copy(h, 0).start()
         hid_copy(h, 1).start()
+
+    def finish(h):
+        from_sibling(h, 1)
+        activate(h)
 
     wide = down_sum.shape[1]
     pieces = result.shape[0]
@@ -896,27 +902,29 @@
     closed(1)
     next_near(0)
     turned(2)
-    far(0)
+    from_sibling(0, 0)
+    finish(0)
     turned(3)
     met(2)
     near(1)
     met(3)
     near(2)
+    from_sibling(1, 0)
+    from_sibling(2, 0)
     loaded(8)
     down_near(0)
+    closed(2)
+    next_near(1)
     loaded(10)
     normalize()
-    for i in range(cuts):
-        share_copy(i, 1).start()
-    closed(2)
-    next_near(1)
-    far(1)
+    finish(1)
     closed(3)
     next_near(2)
     hand_on(0)
-    far(2)
-    for i in range(cuts):
-        share_copy(i, 0).start()
+    finish(2)
+    for kind in (1, 0):
+        for i in range(cuts):
+            share_copy(i, kind).start()
     down_far(0)
     down_near(1)
     hand_on(1)
@@ -929,11 +937,11 @@
         exchange(0, c).start()
     combine(1)
     combine(2)
+    combine(3)
     passed(0)
-    combine(3)
+    combine(0)
     loaded(9)
     mixed(0)
-    combine(0)
     for i in range(1, cuts):
         passed(i)
         mixed(i)
@@ -1030,7 +1038,7 @@
             dma((groups,)),
             dma((groups,)),
             dma((2,)),
-            dma((blocks,)),
+            dma((2 * blocks,)),
             dma((1,)),
             dma((1,)),
             dma((1,)),

time: 38 us -> 37.6 us (0.989)
  Pallas kernels: 37.2 us -> 36.8 us
    pallas_call x1, Pallas kernels: 36.2 us -> 35.7 us  [pair_call(): pl.pallas_call(functools.partial(pair_kernel, groups, parts), out_shape=(...]
where the time goes in v4:
time: 37.6 us; the launch traced here: 37.4 us
  Pallas kernels  36.8 us (98%)
  between operations  0.64 us (2%)
    pallas_call x1, Pallas kernels, pair_call(): pl.pallas_call(functools.partial(pair_kernel, groups, parts), out_shape=(...  35.7 us
    pallas_call x1, Pallas kernels, pair_call(): pl.pallas_call(store, out_shape=(jax.ShapeDtypeStruct((length, out_width)...  1.08 us

profile of v4, /device:TPU:0, one launch (start us, length us, event | category | flops | bytes accessed | tf_op | source)
XLA Modules:
  0.0 37.4 jit_solution(8601193021782723066)
XLA Ops:
  0.6 35.7 %pair_block.1 = (bf16[512,1024]{1,0:T(8,128)(2,1)S(1)}, bf16[2,4,32,512]{3,2,1,0:T(8,128)(2,1)S(1)}, bf16[128,128]{1,0:T(8,128)(2,1)S(1)}) custom-call(bf16[256,512]{1,0:T(8,128)(2,1)} %value_hbm.1, bf16[256,512]{1,0:T(8,128)(2,1)} %gate_hbm.1, bf16[128,4096]{1,0:T(8,128)(2,1)} %input_hbm.1, bf16[1,4096,512]{2,1,0:T(8,128)(2,1)} %wgate_hbm.1, ...), custom_call_target="tpu_custom_call" | custom-call | tf_op jit(solution)/shard_map/pair_block/pallas_call | solution.py:994
  36.3 1.1 %store.1 = (bf16[512,1024]{1,0:T(8,128)(2,1)}, bf16[128,1024]{1,0:T(8,128)(2,1)}) custom-call(bf16[512,1024]{1,0:T(8,128)(2,1)S(1)} %get-tuple-element.5.mixer, bf16[2,4,32,512]{3,2,1,0:T(8,128)(2,1)S(1)} %get-tuple-element.6.returned, bf16[128,128]{1,0:T(8,128)(2,1)S(1)} %get-tuple-element.7.scatter), custom_call_target="tpu_custom_call" | custom-call | tf_op jit(solution)/shard_map/store/pallas_call | solution.py:1061
